TPU v7x, 32 devices: a whole 2x2x4 slice. The times are simulated.
32 devices in a mesh: sp: 8 (over z, y), tp: 4 (over x, core).
Axes of the slice: x: 2, y: 2, z: 4, core: 2. Of those that a mesh axis runs over, the one named last changes fastest.
Arguments:
- frames: bfloat16 [4, 1024, 1024], P('tp', 'sp'), may hold values from -22 to 22
- norm_gain: float32 [1024], replicated, may hold values from 0.5 to 1.5
- conv_value_w: bfloat16 [1024, 512], P(None, 'tp'), may hold values from -0.1875 to 0.1875
- conv_gate_w: bfloat16 [1024, 512], P(None, 'tp'), may hold values from -0.1875 to 0.1875
- conv_taps: bfloat16 [31, 512], P(None, 'tp'), may hold values from -1 to 1
- conv_bias: float32 [512], P('tp'), may hold values from -1.2 to 1.2
- channel_gain: float32 [512], P('tp'), may hold values from 0.5 to 1.5
- channel_shift: float32 [512], P('tp'), may hold values from -1.2 to 1.2
- query_w: bfloat16 [1024, 1024], P(None, 'tp'), may hold values from -0.1875 to 0.1875
- forget_w: bfloat16 [1024, 1024], P(None, 'tp'), may hold values from -0.1875 to 0.1875
- input_w: bfloat16 [1024, 1024], P(None, 'tp'), may hold values from -0.1875 to 0.1875
- gate_w: bfloat16 [1024, 1024], P(None, 'tp'), may hold values from -0.1875 to 0.1875
- memory_rate: float32 [1024], P('tp'), may hold values from 0.5 to 32
- head_gain: float32 [1024], P('tp'), may hold values from 0.5 to 1.5
- conv_out_w: bfloat16 [512, 1024], P('tp'), may hold values from -0.1875 to 0.1875
- rec_out_w: bfloat16 [1024, 1024], P('tp'), may hold values from -0.125 to 0.125
Outputs:
- mixed: bfloat16 [4, 1024, 1024], P('tp', 'sp')
All inputs are finite; a program needn't handle non-finite values.
Results may differ from a plain program's by a relative error of at most 0.015.
The roundings to bfloat16 on the way count: a program that leaves them out, or rounds other values in their place, can miss the bound.
Values may be sent and summed in bfloat16 or wider, within the bound.
No kernel may reach another device: no remote copies, remote signals or barrier semaphores. Data moves between devices by JAX's collectives and lax.ppermute only.
A program may use at most 64 MiB of HBM per device.

v0:
```python
import jax
import jax.numpy as jnp
from jax import lax
from jax.sharding import PartitionSpec as P

D_CONV = 512
HEAD = 128


EPS = 1e-06


def from_behind(value, axis, steps):
    count = lax.axis_size(axis)
    leading, last = (max(0, -steps), min(count, count - steps))
    return lax.ppermute(value, axis, [(source, source + steps) for source in range(leading, last)])


def carried_in(value, axis, join, neutral):
    count, mine = (lax.axis_size(axis), lax.axis_index(axis))
    pieces = jax.tree.map(lambda part: lax.all_gather(part, axis), value)
    total = jax.tree.map(
        lambda part, zero: jnp.full_like(part, 0) + jnp.asarray(zero, part.dtype), value, neutral
    )

    def step(position, total):
        longer = join(total, jax.tree.map(lambda part: part[position], pieces))
        return jax.tree.map(lambda new, old: jnp.where(position < mine, new, old), longer, total)

    return lax.fori_loop(0, count - 1, step, total)


def conv_branch(conv_value, conv_gate, conv_taps, conv_bias, channel_gain, channel_shift):
    gated_conv = (
        conv_value.astype(jnp.float32) * jax.nn.sigmoid(conv_gate.astype(jnp.float32))
    ).astype(jnp.bfloat16)
    positions = gated_conv.shape[1]
    reach_rows = conv_taps.shape[0] - 1
    edge_rows = from_behind(gated_conv[:, positions - reach_rows :, :], "sp", 1)
    extended = jnp.concatenate([edge_rows, gated_conv], axis=1)
    filtered = (
        lax.conv_general_dilated(
            extended,
            conv_taps[:, None, :],
            window_strides=(1,),
            padding=[(0, 0)],
            dimension_numbers=("NWC", "WIO", "NWC"),
            feature_group_count=gated_conv.shape[2],
            preferred_element_type=jnp.float32,
        )
        + conv_bias
    )
    row_sums, row_squares = lax.psum(
        (jnp.sum(filtered, axis=-1), jnp.sum(filtered * filtered, axis=-1)), "tp"
    )
    row_mean = (row_sums / D_CONV)[..., None]
    row_var = (row_squares / D_CONV)[..., None] - row_mean * row_mean
    scaled = (filtered - row_mean) * lax.rsqrt(row_var + EPS) * channel_gain + channel_shift
    return jax.nn.silu(scaled).astype(jnp.bfloat16)


def combine_states(earlier, later):
    return (earlier[0] * later[0], later[0][..., None] * earlier[1] + later[1])


def rec_begin(queries, forget_raw, inputs, memory_rate, seq_total):
    seq_count, positions, rec_local = queries.shape
    head_shape = (seq_count, positions, rec_local // HEAD, HEAD)
    rate_rows = (memory_rate / seq_total).reshape(head_shape[2:])
    in_gate = rate_rows * jax.nn.sigmoid(-forget_raw.astype(jnp.float32)).reshape(head_shape)
    cumulative = jnp.cumsum(jnp.log1p(-in_gate), axis=1)
    final_sum = cumulative[:, -1]
    grown = (queries.astype(jnp.float32).reshape(head_shape) * jnp.exp(cumulative)).astype(
        jnp.bfloat16
    )
    shrunk = (in_gate * jnp.exp(-cumulative)).astype(jnp.bfloat16)
    weighted = (in_gate * jnp.exp(final_sum[:, None] - cumulative)).astype(jnp.bfloat16)
    value_rows = inputs.reshape(head_shape)
    causal = jnp.tril(jnp.ones((positions, positions), dtype=bool))
    scores = jnp.einsum("sthk,suhk->shtu", grown, shrunk, preferred_element_type=jnp.float32)
    scores = jnp.where(causal, scores, 0.0).astype(jnp.bfloat16)
    local_out = jnp.einsum(
        "shtu,suhv->sthv", scores, value_rows, preferred_element_type=jnp.float32
    )
    block_decay = jnp.exp(final_sum)
    block_state = jnp.einsum(
        "suhk,suhv->shkv", weighted, value_rows, preferred_element_type=jnp.float32
    )
    identity = (jnp.ones_like(block_decay), jnp.zeros_like(block_state))
    carried = carried_in((block_decay, block_state), "sp", combine_states, identity)
    return (grown, local_out, carried[1])


def rec_finish(grown, local_out, carried_state, out_gate, head_gain):
    carried_low = carried_state.astype(jnp.bfloat16)
    rec_raw = local_out + jnp.einsum(
        "sthk,shkv->sthv", grown, carried_low, preferred_element_type=jnp.float32
    )
    rec_norm = (
        rec_raw
        * lax.rsqrt(jnp.mean(rec_raw * rec_raw, axis=-1, keepdims=True) + EPS)
        * head_gain.reshape(rec_raw.shape[2:])
    )
    return (rec_norm.reshape(out_gate.shape) * jax.nn.silu(out_gate.astype(jnp.float32))).astype(
        jnp.bfloat16
    )


def local(
    frames,
    norm_gain,
    conv_value_w,
    conv_gate_w,
    conv_taps,
    conv_bias,
    channel_gain,
    channel_shift,
    query_w,
    forget_w,
    input_w,
    gate_w,
    memory_rate,
    head_gain,
    conv_out_w,
    rec_out_w,
):
    values = frames.astype(jnp.float32)
    normed = (
        values * lax.rsqrt(jnp.mean(values * values, axis=-1, keepdims=True) + EPS) * norm_gain
    ).astype(jnp.bfloat16)
    conv_local = conv_value_w.shape[1]
    rec_local = query_w.shape[1]
    joined_weight = jnp.concatenate(
        [conv_value_w, conv_gate_w, query_w, forget_w, input_w, gate_w], axis=1
    )
    product = jnp.einsum(
        "spd,dc->spc",
        lax.all_gather(normed, "tp", axis=0, tiled=True),
        joined_weight,
        preferred_element_type=jnp.float32,
    )
    projected = product.astype(jnp.bfloat16)
    split_points = [
        conv_local,
        2 * conv_local,
        2 * conv_local + rec_local,
        2 * conv_local + 2 * rec_local,
        2 * conv_local + 3 * rec_local,
    ]
    conv_value, conv_gate, queries, forget_raw, inputs, out_gate = jnp.split(
        projected, split_points, axis=-1
    )
    seq_total = frames.shape[1] * lax.axis_size("sp")
    conv_out = conv_branch(conv_value, conv_gate, conv_taps, conv_bias, channel_gain, channel_shift)
    grown, local_out, carried_state = rec_begin(queries, forget_raw, inputs, memory_rate, seq_total)
    rec_out = rec_finish(grown, local_out, carried_state, out_gate, head_gain)
    branches = jnp.concatenate([conv_out, rec_out], axis=-1)
    out_weight = jnp.concatenate([conv_out_w, rec_out_w], axis=0)
    full_rows = lax.all_to_all(branches, "tp", split_axis=0, concat_axis=2, tiled=True)
    full_weight = lax.all_gather(out_weight, "tp", axis=0, tiled=True)
    mixed = jnp.einsum("spc,cd->spd", full_rows, full_weight, preferred_element_type=jnp.float32)
    return mixed.astype(jnp.bfloat16)


def solution(mesh):
    placed = (
        P("tp", "sp", None),
        P(),
        P(None, "tp"),
        P(None, "tp"),
        P(None, "tp"),
        P("tp"),
        P("tp"),
        P("tp"),
        P(None, "tp"),
        P(None, "tp"),
        P(None, "tp"),
        P(None, "tp"),
        P("tp"),
        P("tp"),
        P("tp", None),
        P("tp", None),
    )
    return jax.shard_map(
        local, mesh=mesh, in_specs=placed, out_specs=P("tp", "sp", None), check_vma=False
    )
```

profile of v0, /device:TPU:0, one launch (start us, length us, event | category | flops | bytes accessed | tf_op | source)
XLA Modules:
  0.0 153.3 jit_solution(11214979826300616397)
XLA Ops:
  6.6 1.2 fusion.6
  7.8 1.8 %fusion.8 = bf16[1,128,1024]{2,1,0:T(8,128)(2,1)} fusion(bf16[1,128,1024]{2,1,0:T(8,128)(2,1)} %param.18, f32[1024]{0:T(1024)} %param.19, f32[128]{0:T(128)S(1)} %add_rsqrt_fusion.2), kind=kLoop, calls=%fused_computation.19 | loop fusion | flops 524288 | bytes 528896 | tf_op jit(solution)/shard_map/convert_element_type | solution.py:130
  9.7 1.7 %constant_dynamic-update-slice_fusion.5 = bf16[1024,1280]{1,0:T(8,128)(2,1)} fusion(bf16[1024,128]{1,0:T(8,128)(2,1)} %param.20), kind=kLoop, calls=%fused_computation.66 | loop fusion | bytes 524288
  11.4 1.7 %constant_dynamic-update-slice_fusion.4 = bf16[1024,1280]{1,0:T(8,128)(2,1)} fusion(bf16[1024,1280]{1,0:T(8,128)(2,1)} %constant_dynamic-update-slice_fusion.5, bf16[1024,128]{1,0:T(8,128)(2,1)} %param.21), kind=kLoop, calls=%fused_computation.65 | loop fusion | bytes 524288
  13.1 1.9 %constant_dynamic-update-slice_fusion.3 = bf16[1024,1280]{1,0:T(8,128)(2,1)} fusion(bf16[1024,1280]{1,0:T(8,128)(2,1)} %constant_dynamic-update-slice_fusion.4, bf16[1024,256]{1,0:T(8,128)(2,1)} %param.26), kind=kLoop, calls=%fused_computation.64 | loop fusion | bytes 1048576
  17.7 11.5 %all-gather.6.cloned.1.call-done = bf16[4,128,1024]{2,1,0:T(8,128)(2,1)} async-done(((bf16[1,128,1024]{2,1,0:T(8,128)(2,1)}), bf16[4,128,1024]{2,1,0:T(8,128)(2,1)}) %all-gather.6.cloned.1.call-update) | async-done | bytes 1048592 | tf_op jit(solution)/shard_map/all_gather | solution.py:138
  29.2 3.6 %convolution_convert_fusion = bf16[4,128,1280]{2,1,0:T(8,128)(2,1)S(1)} fusion(bf16[4,128,1024]{2,1,0:T(8,128)(2,1)} %all-gather.6.cloned.1.call-done, bf16[1024,1280]{1,0:T(8,128)(2,1)} %constant_dynamic-update-slice_fusion), kind=kOutput, calls=%fused_computation.3 | convolution fusion | flops 1342832640 | bytes 4980736 | tf_op jit(solution)/shard_map/spd,dc->spc/dot_general | solution.py:136
  36.4 1.1 fusion.19
  39.8 3.4 %collective-permute-start = (bf16[4,30,128]{2,1,0:T(8,128)(2,1)S(1)}, bf16[4,30,128]{2,1,0:T(8,128)(2,1)S(1)}, u32[]{:S(2)}, u32[]{:S(2)}) collective-permute-start(bf16[4,30,128]{2,1,0:T(8,128)(2,1)S(1)} %slice.8), channel_id=1, source_target_pairs={{0,4},{4,8},{8,12},{12,16},{16,20},{20,24},{24,28},{1,5},{5,9},{9,... | collective-permute-start | bytes 92168 | tf_op jit(solution)/shard_map/ppermute | solution.py:16
  43.7 31.6 %all-gather = f32[32,1,2,128]{3,2,1,0:T(2,128)S(1)} all-gather(f32[4,1,2,128]{3,2,1,0:T(2,128)S(1)} %get-tuple-element.138), channel_id=2, replica_groups=mesh['sp'=8,'tp'=4] {'sp'}, dimensions={0}, use_global_device_ids=true | all-gather | bytes 36864 | tf_op jit(solution)/shard_map/all_gather | solution.py:21
  76.3 6.1 %all-reduce = (f32[4,128]{1,0:T(4,128)S(1)}, f32[4,128]{1,0:T(4,128)S(1)}) all-reduce(f32[4,128]{1,0:T(4,128)S(1)} %get-tuple-element.119, f32[4,128]{1,0:T(4,128)S(1)} %get-tuple-element.118), channel_id=1, replica_groups=mesh['sp'=8,'tp'=4] {'tp'}, use_global_device_ids=true, to_apply=%region_4.0 | all-reduce | flops 1024 | bytes 8192 | tf_op jit(solution)/shard_map/psum | solution.py:53
  82.6 28.1 %all-gather.10.cloned.1.call-done = f32[32,2,128,128]{3,2,1,0:T(8,128)} async-done(((f32[4,2,128,128]{3,2,1,0:T(8,128)}), f32[32,2,128,128]{3,2,1,0:T(8,128)}) %all-gather.10.cloned.1.call-update) | async-done | bytes 4194320 | tf_op jit(solution)/shard_map/all_gather | solution.py:21
  110.7 10.1 %while.14 = (s32[]{:T(128)}, f32[4,2,128,128]{3,2,1,0:T(8,128)S(1)}, s32[]{:T(128)}, f32[8,4,2,128]{3,2,1,0:T(2,128)S(1)}, f32[8,4,2,128,128]{4,3,2,1,0:T(8,128)}, /*index=5*/s32[]{:T(128)}, s32[]{:T(128)}) while((s32[]{:T(128)}, f32[4,2,128,128]{3,2,1,0:T(8,128)S(1)}, s32[]{:T(128)}, f32[8,4,2,128]{3,2,1,0:T(2,128)S(1)}, ...), condition=%wide.region_7.8_spmd.clone, body=%wide.region_6.7_spmd.clone.sunk | while | flops 524292 | bytes 1585257 | solution.py:30
  110.7 1.4 fusion.42
  112.2 1.4 fusion.42
  113.6 1.4 fusion.42
  115.0 1.4 fusion.42
  116.4 1.4 fusion.42
  117.9 1.4 fusion.42
  119.4 1.4 fusion.42
  121.5 1.1 fusion.16
  122.7 14.6 %all_to_all.15 = bf16[4,128,384]{2,1,0:T(8,128)(2,1)S(1)} all-to-all(bf16[4,128,384]{2,1,0:T(8,128)(2,1)S(1)} %pad_maximum_fusion.1), channel_id=1, replica_groups=mesh['sp'=8,'tp'=4] {'tp'}, dimensions={0} | all-to-all | bytes 786432 | tf_op jit(solution)/shard_map/all_to_all | solution.py:159
  137.5 6.0 %all-gather.8.cloned.1.call-done = bf16[1536,1024]{1,0:T(8,128)(2,1)} async-done(((bf16[384,1024]{1,0:T(8,128)(2,1)}), bf16[1536,1024]{1,0:T(8,128)(2,1)}) %all-gather.8.cloned.1.call-update) | async-done | bytes 3145744 | tf_op jit(solution)/shard_map/all_gather | solution.py:160
  143.6 3.2 %fusion.4 = bf16[1,128,1024]{2,1,0:T(8,128)(2,1)} fusion(bf16[128,1536]{0,1:T(8,128)(2,1)S(1)} %bitcast.43, bf16[1536,1024]{1,0:T(8,128)(2,1)} %all-gather.8.cloned.1.call-done), kind=kOutput, calls=%fused_computation.10 | convolution fusion | flops 402784256 | bytes 3801088 | tf_op jit(solution)/shard_map/spc,cd->spd/dot_general | solution.py:161
  (67 shorter events, 11.3 us)
Async XLA Ops:
  6.5 68.8 %copy-start = (bf16[31,128]{1,0:T(8,128)(2,1)S(1)}, bf16[31,128]{1,0:T(8,128)(2,1)}, u32[]{:S(2)}) copy-start(bf16[31,128]{1,0:T(8,128)(2,1)} %param.22) | copy-start | bytes 23812
  6.5 8.5 %copy-start.3 = (bf16[1024,256]{1,0:T(8,128)(2,1)S(1)}, bf16[1024,256]{1,0:T(8,128)(2,1)}, u32[]{:S(2)}) copy-start(bf16[1024,256]{1,0:T(8,128)(2,1)} %param.27) | copy-start | bytes 1572868
  6.5 9.3 %copy-start.4 = (bf16[1024,256]{1,0:T(8,128)(2,1)S(1)}, bf16[1024,256]{1,0:T(8,128)(2,1)}, u32[]{:S(2)}) copy-start(bf16[1024,256]{1,0:T(8,128)(2,1)} %param.28) | copy-start | bytes 1572868
  6.5 10.2 %copy-start.5 = (bf16[1024,256]{1,0:T(8,128)(2,1)S(1)}, bf16[1024,256]{1,0:T(8,128)(2,1)}, u32[]{:S(2)}) copy-start(bf16[1024,256]{1,0:T(8,128)(2,1)} %param.29) | copy-start | bytes 1572868
  6.5 22.6 %all-gather.6.cloned.1.call-start = ((), (), s32[]{:S(2)}) async-start(), calls=%async_computation.1 | async-start | bytes 1310720 | tf_op jit(solution)/shard_map/all_gather | solution.py:138
  9.6 8.1 %copy-start.9 = (f32[256]{0:T(256)S(1)}, f32[256]{0:T(256)}, u32[]{:S(2)}) copy-start(f32[256]{0:T(256)} %param.30) | copy-start | bytes 3076
  9.6 101.1 %all-gather.10.cloned.1.call-start = ((), (), s32[]{:S(2)}) async-start(), calls=%async_computation.3 | async-start | bytes 4718592 | tf_op jit(solution)/shard_map/all_gather | solution.py:21
  32.8 1.2 copy-start.1
  35.1 2.4 %copy-start.2 = (bf16[256,1024]{1,0:T(8,128)(2,1)S(1)}, bf16[256,1024]{1,0:T(8,128)(2,1)}, u32[]{:S(2)}) copy-start(bf16[256,1024]{1,0:T(8,128)(2,1)} %param.33) | copy-start | bytes 1572868
  35.1 2.4 %copy-start.6 = (bf16[128,1024]{1,0:T(8,128)(2,1)S(1)}, bf16[128,1024]{1,0:T(8,128)(2,1)}, u32[]{:S(2)}) copy-start(bf16[128,1024]{1,0:T(8,128)(2,1)} %param.32) | copy-start | bytes 786436
  37.5 106.0 %all-gather.8.cloned.1.call-start = ((), (), s32[]{:S(2)}) async-start(), calls=%async_computation.2 | async-start | bytes 3932160 | tf_op jit(solution)/shard_map/all_gather | solution.py:160
  39.8 35.5 %collective-permute-start = (bf16[4,30,128]{2,1,0:T(8,128)(2,1)S(1)}, bf16[4,30,128]{2,1,0:T(8,128)(2,1)S(1)}, u32[]{:S(2)}, u32[]{:S(2)}) collective-permute-start(bf16[4,30,128]{2,1,0:T(8,128)(2,1)S(1)} %slice.8), channel_id=1, source_target_pairs={{0,4},{4,8},{8,12},{12,16},{16,20},{20,24},{24,28},{1,5},{5,9},{9,... | collective-permute-start | bytes 92168 | tf_op jit(solution)/shard_map/ppermute | solution.py:16
  43.6 32.4 %copy-start.7 = (f32[128]{0:T(128)S(1)}, f32[128]{0:T(128)}, u32[]{:S(2)}) copy-start(f32[128]{0:T(128)} %param.23) | copy-start | bytes 1540
  43.7 38.7 %copy-start.10 = (f32[128]{0:T(128)S(1)}, f32[128]{0:T(128)}, u32[]{:S(2)}) copy-start(f32[128]{0:T(128)} %param.25) | copy-start | bytes 1540
  43.7 38.7 %copy-start.11 = (f32[128]{0:T(128)S(1)}, f32[128]{0:T(128)}, u32[]{:S(2)}) copy-start(f32[128]{0:T(128)} %param.24) | copy-start | bytes 1540
  110.7 10.5 %copy-start.8 = (f32[256]{0:T(256)S(1)}, f32[256]{0:T(256)}, u32[]{:S(2)}) copy-start(f32[256]{0:T(256)} %param.31) | copy-start | bytes 3076
Sparse Core Ops, SparseCore 0:
  9.7 19.4 all-gather.5
  37.6 73.0 all-gather.9
  112.3 31.2 all-gather.7
where the time goes:
time: 154 us; the launch traced here: 153 us
  blocking collectives  52.3 us (34%)
  waiting for transfers between devices  45.7 us (30%)
  other arithmetic  18.7 us (12%)
  between operations  13.4 us (9%)
  local copies, waits for them, and re-layouts  10.1 us (7%)
  matrix products  9.42 us (6%)
  starting transfers between devices  3.5 us (2%)
    all_gather x1, blocking collectives, carried_in(): pieces = jax.tree.map(lambda part: lax.all_gather(part, axis), value)  31.6 us
    all_gather x1, waiting for transfers between devices, carried_in(): pieces = jax.tree.map(lambda part: lax.all_gather(part, axis), value)  28.1 us
    all_to_all x1, blocking collectives, local(): lax.all_to_all(branches, 'tp', split_axis=0, concat_axis=2, tiled=True)  14.6 us
    all_gather x1, waiting for transfers between devices, local(): lax.all_gather(normed, 'tp', axis=0, tiled=True)  11.5 us
    select_n x7, other arithmetic, step(): jnp.where(position < mine, new, old)  9.82 us
    unnamed x29, local copies, waits for them, and re-layouts  8.15 us
    psum x1, blocking collectives, conv_branch(): lax.psum((jnp.sum(filtered, axis=-1), jnp.sum(filtered * filtered, axis=-...  6.07 us
    all_gather x1, waiting for transfers between devices, local(): full_weight = lax.all_gather(out_weight, 'tp', axis=0, tiled=True)  6.03 us
  transfers between devices with their start and end apart: 4, of which 3 were waited for; matrix products, arithmetic and copies ran while one was open for 15% of the time, Pallas kernels for 0%

commit v1 on v0

v1 whole, which is shorter than its diff:
```python
import functools
import jax
import jax.numpy as jnp
from jax import lax
from jax.experimental import pallas as pl
from jax.experimental.pallas import tpu as pltpu
from jax.sharding import PartitionSpec as P

HEAD = 128
EPS = 1e-06
EDGE = 32
TAIL = 16
BF16 = jnp.bfloat16
F32 = jnp.float32
AXES = ("sp", "tp")
VMEM_LIMIT = 24 * 1024 * 1024


def route(value, groups, chips, target):
    pairs = []
    for group in range(groups):
        for half in range(2):
            for chip in range(chips):
                for core in range(2):
                    aim = target(group, half, chip, core)
                    if aim is not None:
                        g, h, x, c = aim
                        source = (group * 2 + half) * chips * 2 + chip * 2 + core
                        pairs.append((source, (g * 2 + h) * chips * 2 + x * 2 + c))
    return lax.ppermute(value, AXES, pairs)


def call(body, outs, args, scratch=(), flops=0, size=0):
    spaces = [
        pl.BlockSpec(memory_space=pltpu.SMEM if arg.dtype == jnp.int32 else pltpu.VMEM)
        for arg in args
    ]
    single = not isinstance(outs, (list, tuple))
    shapes = [outs] if single else list(outs)
    result = pl.pallas_call(
        body,
        out_shape=shapes,
        in_specs=spaces,
        out_specs=[pl.BlockSpec(memory_space=pltpu.VMEM)] * len(shapes),
        scratch_shapes=list(scratch),
        compiler_params=pltpu.CompilerParams(vmem_limit_bytes=VMEM_LIMIT),
        cost_estimate=pl.CostEstimate(flops=flops, bytes_accessed=size, transcendentals=0),
    )(*args)
    return result[0] if single else result


def dot(left, right, dims=((1,), (0,)), precision=None):
    return lax.dot_general(
        left, right, (dims, ((), ())), preferred_element_type=F32, precision=precision
    )


def sigmoid(value):
    return 1.0 / (1.0 + jnp.exp(-value))


def begin_kernel(chips, *refs):
    core = refs[0][0]
    pieces = refs[1 : 1 + 2 * chips]
    gain, value_w, gate_w, forget_w, input_w, rate = refs[1 + 2 * chips : 7 + 2 * chips]
    normed_o, gated_o, edge_o, cum_o, in_gate_o, inputs_o, first_o, decay_o, send_o = refs[
        7 + 2 * chips :
    ]
    rows = pieces[0].shape[0]
    heads = rate.shape[1] // HEAD
    lower = lax.broadcasted_iota(jnp.int32, (rows, rows), 1) <= lax.broadcasted_iota(
        jnp.int32, (rows, rows), 0
    )
    lower = lower.astype(F32)
    for k in range(chips):
        mine, other = pieces[2 * k][...], pieces[2 * k + 1][...]
        for half in range(2):
            block = jnp.where(core == half, mine, other).astype(F32)
            scale = lax.rsqrt(jnp.mean(block * block, axis=-1, keepdims=True) + EPS)
            normed_o[k, pl.ds(half * rows, rows), :] = (block * scale * gain[...]).astype(BF16)
        normed = normed_o[k]
        forget_raw = dot(normed, forget_w[...]).astype(BF16).astype(F32)
        inputs = dot(normed, input_w[...]).astype(BF16)
        inputs_o[k] = inputs
        in_gate = rate[...] * sigmoid(-forget_raw)
        in_gate_o[k] = in_gate
        log_forget = jnp.log1p(-in_gate)
        states, lasts = [], []
        for half in range(2):
            part = slice(half * rows, (half + 1) * rows)
            cumulative = dot(lower, log_forget[part], precision=lax.Precision.HIGHEST)
            cum_o[k, pl.ds(half * rows, rows), :] = cumulative
            last = cumulative[rows - 1 : rows]
            weighted = (in_gate[part] * jnp.exp(last - cumulative)).astype(BF16)
            lasts.append(last)
            states.append(
                [
                    dot(
                        inputs[part, h * HEAD : (h + 1) * HEAD],
                        weighted[:, h * HEAD : (h + 1) * HEAD],
                        ((0,), (0,)),
                    )
                    for h in range(heads)
                ]
            )
        decays = [jnp.exp(last) for last in lasts]
        decay_o[k] = jnp.broadcast_to(decays[0], (8, decays[0].shape[1]))
        whole = jnp.exp(lasts[0] + lasts[1])
        high = whole.astype(BF16).astype(F32)
        for h in range(heads):
            cols = slice(h * HEAD, (h + 1) * HEAD)
            first_o[k, h] = states[0][h]
            send_o[k, h, pl.ds(0, HEAD), :] = (
                decays[1][:, cols] * states[0][h] + states[1][h]
            ).astype(BF16)
            spot = lax.broadcasted_iota(jnp.int32, (TAIL, HEAD), 0)
            tail = jnp.where(spot == 0, high[:, cols], (whole - high)[:, cols])
            send_o[k, h, pl.ds(HEAD, TAIL), :] = tail.astype(BF16)
        conv_value = dot(normed, value_w[...]).astype(BF16).astype(F32)
        conv_gate = dot(normed, gate_w[...]).astype(BF16).astype(F32)
        gated = (conv_value * sigmoid(conv_gate)).astype(BF16)
        gated_o[k] = gated
        edge_o[k] = gated[2 * rows - EDGE :]


def middle_kernel(chips, normed, cum, in_gate, inputs, query_w, out_gate_w, *outs):
    grown_o, local_o, gate_o = outs
    rows = normed.shape[1] // 2
    heads = query_w.shape[1] // HEAD
    seen = lax.broadcasted_iota(jnp.int32, (rows, rows), 1) <= lax.broadcasted_iota(
        jnp.int32, (rows, rows), 0
    )
    for k in range(chips):
        queries = dot(normed[k], query_w[...]).astype(BF16).astype(F32)
        gate_o[k] = dot(normed[k], out_gate_w[...]).astype(BF16)
        growth = jnp.exp(cum[k])
        grown = (queries * growth).astype(BF16)
        shrunk = (in_gate[k] * jnp.exp(-cum[k])).astype(BF16)
        grown_o[k] = grown
        for half in range(2):
            part = slice(half * rows, (half + 1) * rows)
            for h in range(heads):
                cols = slice(h * HEAD, (h + 1) * HEAD)
                scores = dot(grown[part, cols], shrunk[part, cols], ((1,), (1,)))
                scores = jnp.where(seen, scores, 0.0).astype(BF16)
                local_o[k, pl.ds(half * rows, rows), pl.ds(h * HEAD, HEAD)] = dot(
                    scores, inputs[k, pl.ds(half * rows, rows), pl.ds(h * HEAD, HEAD)]
                )


def conv_kernel(chips, core, gated, edge, taps, bias, gain, shift, *refs):
    outs, extended = refs[:-1], refs[-1]
    rows = gated.shape[1] // 2
    width = taps.shape[0]
    for k in range(chips):
        extended[pl.ds(0, EDGE), :] = edge[k].astype(F32)
        extended[pl.ds(EDGE, 2 * rows), :] = gated[k].astype(F32)
        for half in range(2):
            total = jnp.broadcast_to(bias[...], (rows, bias.shape[1]))
            for j in range(width):
                start = half * rows + EDGE - (width - 1) + j
                total = total + taps[pl.ds(j, 1), :].astype(F32) * extended[pl.ds(start, rows), :]
            for e in range(2):
                @pl.when((core[0] ^ e) == half)
                def _():
                    outs[2 * k + e][pl.ds(0, rows), :] = total
        spot = lax.broadcasted_iota(jnp.int32, (8, bias.shape[1]), 0)
        for e in range(2):
            outs[2 * k + e][pl.ds(rows, 8), :] = jnp.where(spot == 0, gain[...], shift[...])


def finish_kernel(chips, core, *refs):
    arrived = refs[: -6 - 2 * chips]
    first, decay, grown, local, out_gate, gain = refs[-6 - 2 * chips : -2 * chips]
    outs = refs[-2 * chips :]
    rows = grown.shape[1] // 2
    heads = gain.shape[1] // HEAD
    for k in range(chips):
        for h in range(heads):
            cols = slice(h * HEAD, (h + 1) * HEAD)
            state, span = None, None
            for ref in arrived:
                part = ref[k, h, pl.ds(0, HEAD), :].astype(F32)
                ends = ref[k, h, pl.ds(HEAD, TAIL), :].astype(F32)
                ends = ends[0:1] + ends[1:2]
                state = part if state is None else state + span * part
                span = ends if span is None else span * ends
            later = decay[k, 0:1, cols] * state + first[k, h]
            for e in range(2):
                half = core[0] ^ e
                low = jnp.where(half == 0, state, later).astype(BF16)
                part = pl.ds(pl.multiple_of(half * rows, rows), rows)
                raw = local[k, part, cols] + dot(grown[k, part, cols], low, ((1,), (1,)))
                scale = lax.rsqrt(jnp.mean(raw * raw, axis=-1, keepdims=True) + EPS)
                gate = out_gate[k, part, cols].astype(F32)
                outs[2 * k + e][:, cols] = (
                    raw * scale * gain[:, cols] * (gate * sigmoid(gate))
                ).astype(BF16)


def sorted_pair(swap, first, second):
    return jnp.where(swap, second, first), jnp.where(swap, first, second)


def conv_out_kernel(chips, where, *refs):
    parts, weights, out = refs[: 2 * chips], refs[2 * chips : 4 * chips], refs[4 * chips]
    rows = parts[0].shape[0] - 8
    channels = 2 * chips * parts[0].shape[1]
    values = [part[pl.ds(0, rows), :] for part in parts]
    total = sum(jnp.sum(value, axis=-1, keepdims=True) for value in values)
    square = sum(jnp.sum(value * value, axis=-1, keepdims=True) for value in values)
    mean = total / channels
    scale = lax.rsqrt(square / channels - mean * mean + EPS)
    result = []
    for part, value in zip(parts, values):
        tail = part[pl.ds(rows, 8), :]
        scaled = (value - mean) * scale * tail[0:1] + tail[1:2]
        result.append(scaled * sigmoid(scaled))
    swap = where[0] != where[1]
    total = None
    for k in range(chips):
        near, far = sorted_pair(swap, result[2 * k], result[2 * k + 1])
        term = dot(near.astype(BF16), weights[2 * k][...]) + dot(
            far.astype(BF16), weights[2 * k + 1][...]
        )
        total = term if total is None else total + term
    out[...] = total


def rec_out_kernel(chips, where, conv_part, *refs):
    parts, weights, out = refs[: 2 * chips], refs[2 * chips : 4 * chips], refs[4 * chips]
    swap = where[0] != where[1]
    total = conv_part[...]
    for k in range(chips):
        near, far = sorted_pair(swap, parts[2 * k][...], parts[2 * k + 1][...])
        total = total + dot(near, weights[2 * k][...]) + dot(far, weights[2 * k + 1][...])
    out[...] = total.astype(BF16)


def local(
    frames,
    norm_gain,
    conv_value_w,
    conv_gate_w,
    conv_taps,
    conv_bias,
    channel_gain,
    channel_shift,
    query_w,
    forget_w,
    input_w,
    gate_w,
    memory_rate,
    head_gain,
    conv_out_w,
    rec_out_w,
):
    assert frames.shape[0] == 1
    groups, chips = lax.axis_size("sp") // 2, lax.axis_size("tp") // 2
    rows, width = frames.shape[1:]
    conv_local, rec_local = conv_value_w.shape[1], query_w.shape[1]
    heads = rec_local // HEAD
    seq_total = rows * lax.axis_size("sp")
    half = (lax.axis_index("sp") % 2).astype(jnp.int32)
    core = (lax.axis_index("tp") % 2).astype(jnp.int32)
    core_s = core.reshape(1)
    where_s = jnp.stack([half, core])
    send = functools.partial(route, groups=groups, chips=chips)
    shape = jax.ShapeDtypeStruct

    def partner(value):
        return send(value, target=lambda g, h, x, c: (g, h, x, 1 - c))

    def shifted(value, k):
        return send(value, target=lambda g, h, x, c: (g, h, (x + k) % chips, c))

    pieces = []
    flat = frames[0]
    for k in range(chips):
        mine = send(flat, target=lambda g, h, x, c: (g, c, (x + k) % chips, h))
        pieces += [mine, partner(mine)]

    conv_weights, rec_weights = [], []
    for k in range(chips):
        for weight, kept in ((conv_out_w, conv_weights), (rec_out_w, rec_weights)):
            near = weight if k == 0 else shifted(weight, k)
            kept += [near, partner(near)]

    row = lambda vector: vector.reshape(1, -1)
    span = 2 * rows
    normed, gated, edge, cum, in_gate, inputs, first, decay, packet = call(
        functools.partial(begin_kernel, chips),
        [
            shape((chips, span, width), BF16),
            shape((chips, span, conv_local), BF16),
            shape((chips, EDGE, conv_local), BF16),
            shape((chips, span, rec_local), F32),
            shape((chips, span, rec_local), F32),
            shape((chips, span, rec_local), BF16),
            shape((chips, heads, HEAD, HEAD), F32),
            shape((chips, 8, rec_local), F32),
            shape((chips, heads, HEAD + TAIL, HEAD), BF16),
        ],
        [core_s, *pieces, row(norm_gain), conv_value_w, conv_gate_w, forget_w, input_w,
         row(memory_rate / seq_total)],
        flops=2 * chips * span * width * (2 * conv_local + 2 * rec_local),
        size=1 << 21,
    )

    def later(value, steps):
        return send(
            value,
            target=lambda g, h, x, c: (g + steps, h, x, c) if g + steps < groups else None,
        )

    before = later(edge, 1)
    arrived = [later(packet, steps) for steps in range(1, groups)]

    grown, local_out, out_gate = call(
        functools.partial(middle_kernel, chips),
        [
            shape((chips, span, rec_local), BF16),
            shape((chips, span, rec_local), F32),
            shape((chips, span, rec_local), BF16),
        ],
        [normed, cum, in_gate, inputs, query_w, gate_w],
        flops=2 * chips * span * width * 2 * rec_local,
        size=1 << 21,
    )
    filtered = call(
        functools.partial(conv_kernel, chips),
        [shape((rows + 8, conv_local), F32)] * (2 * chips),
        [core_s, gated, before, conv_taps, row(conv_bias), row(channel_gain), row(channel_shift)],
        scratch=[pltpu.VMEM((span + EDGE, conv_local), F32)],
        flops=1 << 28,
        size=1 << 20,
    )

    def home(parts):
        result = []
        for k in range(chips):
            for e in range(2):
                part = parts[2 * ((chips - k) % chips) + e]
                result.append(
                    send(part, target=lambda g, h, x, c: (g, c ^ e, (x + k) % chips, h))
                )
        return result

    conv_part = call(
        functools.partial(conv_out_kernel, chips),
        shape((rows, width), F32),
        [where_s, *home(filtered), *conv_weights],
        flops=2 * rows * width * 2 * chips * conv_local,
        size=1 << 20,
    )
    rec_out = call(
        functools.partial(finish_kernel, chips),
        [shape((rows, rec_local), BF16)] * (2 * chips),
        [core_s, *arrived, first, decay, grown, local_out, out_gate, row(head_gain)],
        flops=1 << 28,
        size=1 << 21,
    )
    mixed = call(
        functools.partial(rec_out_kernel, chips),
        shape((rows, width), BF16),
        [where_s, conv_part, *home(rec_out), *rec_weights],
        flops=2 * rows * width * 2 * chips * rec_local,
        size=1 << 21,
    )
    return mixed[None]


def solution(mesh):
    placed = (
        P("tp", "sp", None),
        P(),
        P(None, "tp"),
        P(None, "tp"),
        P(None, "tp"),
        P("tp"),
        P("tp"),
        P("tp"),
        P(None, "tp"),
        P(None, "tp"),
        P(None, "tp"),
        P(None, "tp"),
        P("tp"),
        P("tp"),
        P("tp", None),
        P("tp", None),
    )
    return jax.shard_map(
        local, mesh=mesh, in_specs=placed, out_specs=P("tp", "sp", None), check_vma=False
    )
```

time: 154 us -> 87.4 us (0.57)
  blocking collectives: 52.3 us -> 0 us
  starting transfers between devices: 3.5 us -> 38.1 us
  waiting for transfers between devices: 45.7 us -> 16.2 us
  other arithmetic: 18.7 us -> 0.08 us
  between operations: 13.4 us -> 0.2 us
  Pallas kernels: 0 us -> 11.8 us
  local copies, waits for them, and re-layouts: 10.1 us -> 20.2 us
  matrix products: 9.42 us -> 0 us
    all_gather x3 -> x0, waiting for transfers between devices: 45.7 us -> none  [the longest x1 28.1 us: carried_in(): pieces = jax.tree.map(lambda part: lax.all_gather(part, axis), value)]
    ppermute x1 -> x22, starting transfers between devices: 3.38 us -> 38.1 us  [route(): return lax.ppermute(value, AXES, pairs)]
    all_gather x1 -> x0, blocking collectives: 31.6 us -> none  [carried_in(): pieces = jax.tree.map(lambda part: lax.all_gather(part, axis), value)]
    ppermute x1 -> x22, waiting for transfers between devices: 0.01 us -> 16.2 us  [route(): return lax.ppermute(value, AXES, pairs)]
    all_to_all x1 -> x0, blocking collectives: 14.6 us -> none  [local(): lax.all_to_all(branches, 'tp', split_axis=0, concat_axis=2, tiled=True)]
    unnamed x29 -> x66, local copies, waits for them, and re-layouts: 8.15 us -> 20.2 us
    pallas_call x0 -> x6, Pallas kernels: none -> 11.8 us  [call(): pl.pallas_call(body, out_shape=shapes, in_specs=spaces, out_specs=[pl.Blo...]
    select_n x7 -> x0, other arithmetic: 9.82 us -> none  [step(): jnp.where(position < mine, new, old)]
  transfers between devices with their start and end apart: 4 -> 22, of which waited for: 3 -> 4; matrix products, arithmetic and copies ran while one was open for 15% -> 0% of each run, Pallas kernels for 0% -> 11%
where the time goes in v1:
time: 87.4 us; the launch traced here: 86.6 us
  starting transfers between devices  38.1 us (44%)
  local copies, waits for them, and re-layouts  20.2 us (23%)
  waiting for transfers between devices  16.2 us (19%)
  Pallas kernels  11.8 us (14%)
    ppermute x22, starting transfers between devices, route(): return lax.ppermute(value, AXES, pairs)  38.1 us
    unnamed x66, local copies, waits for them, and re-layouts  20.2 us
    ppermute x22, waiting for transfers between devices, route(): return lax.ppermute(value, AXES, pairs)  16.2 us
    pallas_call x6, Pallas kernels, call(): pl.pallas_call(body, out_shape=shapes, in_specs=spaces, out_specs=[pl.Blo...  11.8 us
  transfers between devices with their start and end apart: 22, of which 4 were waited for; matrix products, arithmetic and copies ran while one was open for 0% of the time, Pallas kernels for 11%

profile of v1, /device:TPU:0, one launch (start us, length us, event | category | flops | bytes accessed | tf_op | source)
XLA Modules:
  0.0 86.6 jit_solution(455398803789307600)
XLA Ops:
  0.0 1.7 %collective-permute-start = (bf16[128,1024]{1,0:T(8,128)(2,1)}, bf16[128,1024]{1,0:T(8,128)(2,1)S(1)}, u32[]{:S(2)}, u32[]{:S(2)}) collective-permute-start(bf16[128,1024]{1,0:T(8,128)(2,1)} %bitcast.16), channel_id=1, source_target_pairs={{0,0},{1,4},{2,2},{3,6},{4,1},{5,5},{6,3},{7,7},{8,8},{9,12},{10,1... | collective-permute-start | bytes 786440 | tf_op jit(solution)/shard_map/ppermute | solution.py:30
  1.7 3.0 %collective-permute-start.20 = (bf16[256,1024]{1,0:T(8,128)(2,1)}, bf16[256,1024]{1,0:T(8,128)(2,1)S(1)}, u32[]{:S(2)}, u32[]{:S(2)}) collective-permute-start(bf16[256,1024]{1,0:T(8,128)(2,1)} %refs_4_.3), channel_id=1, source_target_pairs={{0,2},{1,3},{2,0},{3,1},{4,6},{5,7},{6,4},{7,5},{8,10},{9,11},{10,... | collective-permute-start | bytes 1572872 | tf_op jit(solution)/shard_map/ppermute | solution.py:30
  4.7 2.0 %collective-permute-start.10 = (bf16[128,1024]{1,0:T(8,128)(2,1)}, bf16[128,1024]{1,0:T(8,128)(2,1)}, u32[]{:S(2)}, u32[]{:S(2)}) collective-permute-start(bf16[128,1024]{1,0:T(8,128)(2,1)} %refs_4_.2), channel_id=1, source_target_pairs={{0,2},{1,3},{2,0},{3,1},{4,6},{5,7},{6,4},{7,5},{8,10},{9,11},{10,... | collective-permute-start | bytes 786440 | tf_op jit(solution)/shard_map/ppermute | solution.py:30
  6.7 3.0 %collective-permute-start.1 = (bf16[128,1024]{1,0:T(8,128)(2,1)S(1)}, bf16[128,1024]{1,0:T(8,128)(2,1)S(1)}, u32[]{:S(2)}, u32[]{:S(2)}) collective-permute-start(bf16[128,1024]{1,0:T(8,128)(2,1)S(1)} %collective-permute-done.refs_1_), channel_id=1, source_target_pairs={{0,1},{1,0},{2,3},{3,2},{4,5},{5,4},{6,7},{7,6},{8,9},{9,8},{10,11... | collective-permute-start | bytes 786440 | tf_op jit(solution)/shard_map/ppermute | solution.py:30
  9.7 12.2 %collective-permute-done.2.refs_3_ = bf16[128,1024]{1,0:T(8,128)(2,1)S(1)} collective-permute-done((bf16[128,1024]{1,0:T(8,128)(2,1)}, bf16[128,1024]{1,0:T(8,128)(2,1)S(1)}, u32[]{:S(2)}, u32[]{:S(2)}) %collective-permute-start.2) | collective-permute-done | bytes 262176 | tf_op jit(solution)/shard_map/ppermute | solution.py:30
  21.9 3.1 %collective-permute-start.3 = (bf16[128,1024]{1,0:T(8,128)(2,1)S(1)}, bf16[128,1024]{1,0:T(8,128)(2,1)S(1)}, u32[]{:S(2)}, u32[]{:S(2)}) collective-permute-start(bf16[128,1024]{1,0:T(8,128)(2,1)S(1)} %collective-permute-done.2.refs_3_), channel_id=1, source_target_pairs={{0,1},{1,0},{2,3},{3,2},{4,5},{5,4},{6,7},{7,6},{8,9},{9,8},{10,11... | collective-permute-start | bytes 786440 | tf_op jit(solution)/shard_map/ppermute | solution.py:30
  25.7 1.8 %collective-permute-done.10.refs_6_ = bf16[128,1024]{1,0:T(8,128)(2,1)} collective-permute-done((bf16[128,1024]{1,0:T(8,128)(2,1)}, bf16[128,1024]{1,0:T(8,128)(2,1)}, u32[]{:S(2)}, u32[]{:S(2)}) %collective-permute-start.10) | collective-permute-done | bytes 262176 | tf_op jit(solution)/shard_map/ppermute | solution.py:30
  27.5 1.3 %collective-permute-start.9 = (bf16[128,1024]{1,0:T(8,128)(2,1)}, bf16[128,1024]{1,0:T(8,128)(2,1)}, u32[]{:S(2)}, u32[]{:S(2)}) collective-permute-start(bf16[128,1024]{1,0:T(8,128)(2,1)} %refs_4_.2), channel_id=1, source_target_pairs={{0,1},{1,0},{2,3},{3,2},{4,5},{5,4},{6,7},{7,6},{8,9},{9,8},{10,11... | collective-permute-start | bytes 786440 | tf_op jit(solution)/shard_map/ppermute | solution.py:30
  30.8 1.0 %copy-done.13 = bf16[1024,256]{1,0:T(8,128)(2,1)S(1)} copy-done((bf16[1024,256]{1,0:T(8,128)(2,1)S(1)}, bf16[1024,256]{1,0:T(8,128)(2,1)}, u32[]{:S(2)}) %copy-start.13) | copy-done | bytes 524312
  31.8 1.0 %copy-done.14 = bf16[1024,256]{1,0:T(8,128)(2,1)S(1)} copy-done((bf16[1024,256]{1,0:T(8,128)(2,1)S(1)}, bf16[1024,256]{1,0:T(8,128)(2,1)}, u32[]{:S(2)}) %copy-start.14) | copy-done | bytes 524312
  37.6 3.9 %shard_map.154 = (bf16[2,256,1024]{2,1,0:T(8,128)(2,1)S(1)}, bf16[2,256,128]{2,1,0:T(8,128)(2,1)S(1)}, bf16[2,32,128]{2,1,0:T(8,128)(2,1)S(1)}, f32[2,256,256]{2...) custom-call(s32[1]{0:T(128)} %bitcast.1.refs_0_.core, ...), custom_call_target="tpu_custom_call" | custom-call | flops 805306368 | bytes 2097152 | tf_op jit(solution)/shard_map/pallas_call | solution.py:40
  45.0 4.1 %collective-permute-start.4 = (bf16[2,32,128]{2,1,0:T(8,128)(2,1)S(1)}, bf16[2,32,128]{2,1,0:T(8,128)(2,1)S(1)}, u32[]{:S(2)}, u32[]{:S(2)}) collective-permute-start(bf16[2,32,128]{2,1,0:T(8,128)(2,1)S(1)} %get-tuple-element.26), channel_id=1, source_target_pairs={{0,8},{1,9},{2,10},{3,11},{4,12},{5,13},{6,14},{7,15},{8,16},{9,17... | collective-permute-start | bytes 49160 | tf_op jit(solution)/shard_map/ppermute | solution.py:30
  49.2 3.5 %collective-permute-start.12 = (bf16[2,2,144,128]{3,2,1,0:T(8,128)(2,1)}, bf16[2,2,144,128]{3,2,1,0:T(8,128)(2,1)S(1)}, u32[]{:S(2)}, u32[]{:S(2)}) collective-permute-start(bf16[2,2,144,128]{3,2,1,0:T(8,128)(2,1)} %get-tuple-element.31), channel_id=1, source_target_pairs={{0,8},{1,9},{2,10},{3,11},{4,12},{5,13},{6,14},{7,15},{8,16},{9,17... | collective-permute-start | bytes 442376 | tf_op jit(solution)/shard_map/ppermute | solution.py:30
  52.7 3.6 %collective-permute-start.13 = (bf16[2,2,144,128]{3,2,1,0:T(8,128)(2,1)}, bf16[2,2,144,128]{3,2,1,0:T(8,128)(2,1)}, u32[]{:S(2)}, u32[]{:S(2)}) collective-permute-start(bf16[2,2,144,128]{3,2,1,0:T(8,128)(2,1)} %get-tuple-element.31), channel_id=1, source_target_pairs={{0,16},{1,17},{2,18},{3,19},{4,20},{5,21},{6,22},{7,23},{8,24},{9,... | collective-permute-start | bytes 442376 | tf_op jit(solution)/shard_map/ppermute | solution.py:30
  56.9 1.9 %collective-permute-start.14 = (bf16[2,2,144,128]{3,2,1,0:T(8,128)(2,1)}, bf16[2,2,144,128]{3,2,1,0:T(8,128)(2,1)}, u32[]{:S(2)}, u32[]{:S(2)}) collective-permute-start(bf16[2,2,144,128]{3,2,1,0:T(8,128)(2,1)} %get-tuple-element.31), channel_id=1, source_target_pairs={{0,24},{1,25},{2,26},{3,27},{4,28},{5,29},{6,30},{7,31}} | collective-permute-start | bytes 442376 | tf_op jit(solution)/shard_map/ppermute | solution.py:30
  64.5 2.4 %collective-permute-start.6 = (f32[136,128]{1,0:T(8,128)S(1)}, f32[136,128]{1,0:T(8,128)S(1)}, u32[]{:S(2)}, u32[]{:S(2)}) collective-permute-start(f32[136,128]{1,0:T(8,128)S(1)} %get-tuple-element.28), channel_id=1, source_target_pairs={{0,4},{1,0},{2,6},{3,2},{4,5},{5,1},{6,7},{7,3},{8,12},{9,8},{10,1... | collective-permute-start | bytes 208904 | tf_op jit(solution)/shard_map/ppermute | solution.py:30
  66.8 1.5 %collective-permute-start.7 = (f32[136,128]{1,0:T(8,128)S(1)}, f32[136,128]{1,0:T(8,128)S(1)}, u32[]{:S(2)}, u32[]{:S(2)}) collective-permute-start(f32[136,128]{1,0:T(8,128)S(1)} %get-tuple-element.29), channel_id=1, source_target_pairs={{0,2},{1,6},{2,0},{3,4},{4,3},{5,7},{6,1},{7,5},{8,10},{9,14},{10,... | collective-permute-start | bytes 208904 | tf_op jit(solution)/shard_map/ppermute | solution.py:30
  71.2 1.8 %shard_map.157 = (bf16[2,256,256]{2,1,0:T(8,128)(2,1)S(1)}, f32[2,256,256]{2,1,0:T(8,128)S(1)}, bf16[2,256,256]{2,1,0:T(8,128)(2,1)S(1)}) custom-call(bf16[2,256,1024]{2,1,0:T(8,128)(2,1)S(1)} %get-tuple-element.34.normed, f32[2,256,256]{2,1,0:T(8,128)S(1)} %copy-done.4, f32[2,256,256]{2,1,0:T(8,128)S(1)} %copy-done.6, bf16[2,256,256]{2,1,0:T(8,128)(2,1)S(1)} %copy-done.9, ...), custom_call_target="tpu_custom_call" | custom-call | flops 536870912 | bytes 2097152 | tf_op jit(solution)/shard_map/pallas_call | solution.py:40
  73.6 1.5 %shard_map.158 = (bf16[128,256]{1,0:T(8,128)(2,1)S(1)}, bf16[128,256]{1,0:T(8,128)(2,1)S(1)}, bf16[128,256]{1,0:T(8,128)(2,1)S(1)}, bf16[128,256]{1,0:T(8,128)(2,1)S(1)}) custom-call(s32[1]{0:T(128)} %bitcast.1.refs_0_.core, bf16[2,2,144,128]{3,2,1,0:T(8,128)(2,1)S(1)} %collective-permute-done.12.refs_0_, ...), custom_call_target="tpu_custom_call" | custom-call | flops 268435456 | bytes 2097152 | tf_op jit(solution)/shard_map/pallas_call | solution.py:40
  75.9 2.8 %collective-permute-start.16 = (bf16[128,256]{1,0:T(8,128)(2,1)S(1)}, bf16[128,256]{1,0:T(8,128)(2,1)S(1)}, u32[]{:S(2)}, u32[]{:S(2)}) collective-permute-start(bf16[128,256]{1,0:T(8,128)(2,1)S(1)} %get-tuple-element.42), channel_id=1, source_target_pairs={{0,4},{1,0},{2,6},{3,2},{4,5},{5,1},{6,7},{7,3},{8,12},{9,8},{10,1... | collective-permute-start | bytes 196616 | tf_op jit(solution)/shard_map/ppermute | solution.py:30
  78.7 1.5 %collective-permute-start.17 = (bf16[128,256]{1,0:T(8,128)(2,1)S(1)}, bf16[128,256]{1,0:T(8,128)(2,1)S(1)}, u32[]{:S(2)}, u32[]{:S(2)}) collective-permute-start(bf16[128,256]{1,0:T(8,128)(2,1)S(1)} %get-tuple-element.43), channel_id=1, source_target_pairs={{0,2},{1,6},{2,0},{3,4},{4,3},{5,7},{6,1},{7,5},{8,10},{9,14},{10,... | collective-permute-start | bytes 196616 | tf_op jit(solution)/shard_map/ppermute | solution.py:30
  80.4 1.8 %shard_map.156.conv_part = f32[128,1024]{1,0:T(8,128)S(1)} custom-call(s32[2]{0:T(128)S(1)} %pad_add_fusion.where, f32[136,128]{1,0:T(8,128)S(1)} %collective-permute-done.5.refs_0_, f32[136,128]{1,0:T(8,128)S(1)} %collective-permute-done.6.refs_1_, f32[136,128]{1,0:T(8,128)S(1)} %collective-permute-done.7.refs_2_, ...), custom_call_target="tpu_custom_call" | custom-call | flops 134217728 | bytes 1048576 | tf_op jit(solution)/shard_map/pallas_call | solution.py:40
  82.9 1.4 %collective-permute-done.18.refs_3_ = bf16[128,256]{1,0:T(8,128)(2,1)S(1)} collective-permute-done((bf16[128,256]{1,0:T(8,128)(2,1)S(1)}, bf16[128,256]{1,0:T(8,128)(2,1)S(1)}, u32[]{:S(2)}, u32[]{:S(2)}) %collective-permute-start.18) | collective-permute-done | bytes 65568 | tf_op jit(solution)/shard_map/ppermute | solution.py:30
  84.4 2.2 %shard_map.159 = bf16[128,1024]{1,0:T(8,128)(2,1)} custom-call(s32[2]{0:T(128)S(1)} %pad_add_fusion.where, f32[128,1024]{1,0:T(8,128)S(1)} %shard_map.156.conv_part, bf16[128,256]{1,0:T(8,128)(2,1)S(1)} %collective-permute-done.15.refs_0_, bf16[128,256]{1,0:T(8,128)(2,1)S(1)} %collective-permute-done.16.refs_1_, ...), custom_call_target="tpu_custom_call" | custom-call | flops 268435456 | bytes 2097152 | tf_op jit(solution)/shard_map/pallas_call | solution.py:40
  (94 shorter events, 22.3 us)
Async XLA Ops:
  0.0 30.1 %copy-start.32 = (f32[256]{0:T(256)S(1)}, f32[256]{0:T(256)}, u32[]{:S(2)}) copy-start(f32[256]{0:T(256)} %param.28) | copy-start | bytes 3076
  0.0 6.7 %collective-permute-start = (bf16[128,1024]{1,0:T(8,128)(2,1)}, bf16[128,1024]{1,0:T(8,128)(2,1)S(1)}, u32[]{:S(2)}, u32[]{:S(2)}) collective-permute-start(bf16[128,1024]{1,0:T(8,128)(2,1)} %bitcast.16), channel_id=1, source_target_pairs={{0,0},{1,4},{2,2},{3,6},{4,1},{5,5},{6,3},{7,7},{8,8},{9,12},{10,1... | collective-permute-start | bytes 786440 | tf_op jit(solution)/shard_map/ppermute | solution.py:30
  1.7 27.8 %collective-permute-start.20 = (bf16[256,1024]{1,0:T(8,128)(2,1)}, bf16[256,1024]{1,0:T(8,128)(2,1)S(1)}, u32[]{:S(2)}, u32[]{:S(2)}) collective-permute-start(bf16[256,1024]{1,0:T(8,128)(2,1)} %refs_4_.3), channel_id=1, source_target_pairs={{0,2},{1,3},{2,0},{3,1},{4,6},{5,7},{6,4},{7,5},{8,10},{9,11},{10,... | collective-permute-start | bytes 1572872 | tf_op jit(solution)/shard_map/ppermute | solution.py:30
  4.7 17.2 %collective-permute-start.2 = (bf16[128,1024]{1,0:T(8,128)(2,1)}, bf16[128,1024]{1,0:T(8,128)(2,1)S(1)}, u32[]{:S(2)}, u32[]{:S(2)}) collective-permute-start(bf16[128,1024]{1,0:T(8,128)(2,1)} %bitcast.17), channel_id=1, source_target_pairs={{0,2},{1,6},{2,0},{3,4},{4,3},{5,7},{6,1},{7,5},{8,10},{9,14},{10,... | collective-permute-start | bytes 786440 | tf_op jit(solution)/shard_map/ppermute | solution.py:30
  4.7 22.8 %collective-permute-start.10 = (bf16[128,1024]{1,0:T(8,128)(2,1)}, bf16[128,1024]{1,0:T(8,128)(2,1)}, u32[]{:S(2)}, u32[]{:S(2)}) collective-permute-start(bf16[128,1024]{1,0:T(8,128)(2,1)} %refs_4_.2), channel_id=1, source_target_pairs={{0,2},{1,3},{2,0},{3,1},{4,6},{5,7},{6,4},{7,5},{8,10},{9,11},{10,... | collective-permute-start | bytes 786440 | tf_op jit(solution)/shard_map/ppermute | solution.py:30
  6.7 22.1 %collective-permute-start.1 = (bf16[128,1024]{1,0:T(8,128)(2,1)S(1)}, bf16[128,1024]{1,0:T(8,128)(2,1)S(1)}, u32[]{:S(2)}, u32[]{:S(2)}) collective-permute-start(bf16[128,1024]{1,0:T(8,128)(2,1)S(1)} %collective-permute-done.refs_1_), channel_id=1, source_target_pairs={{0,1},{1,0},{2,3},{3,2},{4,5},{5,4},{6,7},{7,6},{8,9},{9,8},{10,11... | collective-permute-start | bytes 786440 | tf_op jit(solution)/shard_map/ppermute | solution.py:30
  9.7 54.1 %collective-permute-start.19 = (bf16[256,1024]{1,0:T(8,128)(2,1)}, bf16[256,1024]{1,0:T(8,128)(2,1)S(1)}, u32[]{:S(2)}, u32[]{:S(2)}) collective-permute-start(bf16[256,1024]{1,0:T(8,128)(2,1)} %refs_4_.3), channel_id=1, source_target_pairs={{0,1},{1,0},{2,3},{3,2},{4,5},{5,4},{6,7},{7,6},{8,9},{9,8},{10,11... | collective-permute-start | bytes 1572872 | tf_op jit(solution)/shard_map/ppermute | solution.py:30
  21.9 8.2 %collective-permute-start.3 = (bf16[128,1024]{1,0:T(8,128)(2,1)S(1)}, bf16[128,1024]{1,0:T(8,128)(2,1)S(1)}, u32[]{:S(2)}, u32[]{:S(2)}) collective-permute-start(bf16[128,1024]{1,0:T(8,128)(2,1)S(1)} %collective-permute-done.2.refs_3_), channel_id=1, source_target_pairs={{0,1},{1,0},{2,3},{3,2},{4,5},{5,4},{6,7},{7,6},{8,9},{9,8},{10,11... | collective-permute-start | bytes 786440 | tf_op jit(solution)/shard_map/ppermute | solution.py:30
  27.5 21.7 %collective-permute-start.9 = (bf16[128,1024]{1,0:T(8,128)(2,1)}, bf16[128,1024]{1,0:T(8,128)(2,1)}, u32[]{:S(2)}, u32[]{:S(2)}) collective-permute-start(bf16[128,1024]{1,0:T(8,128)(2,1)} %refs_4_.2), channel_id=1, source_target_pairs={{0,1},{1,0},{2,3},{3,2},{4,5},{5,4},{6,7},{7,6},{8,9},{9,8},{10,11... | collective-permute-start | bytes 786440 | tf_op jit(solution)/shard_map/ppermute | solution.py:30
  29.6 23.2 %collective-permute-start.11 = (bf16[128,1024]{1,0:T(8,128)(2,1)}, bf16[128,1024]{1,0:T(8,128)(2,1)}, u32[]{:S(2)}, u32[]{:S(2)}) collective-permute-start(bf16[128,1024]{1,0:T(8,128)(2,1)} %collective-permute-done.10.refs_6_), channel_id=1, source_target_pairs={{0,1},{1,0},{2,3},{3,2},{4,5},{5,4},{6,7},{7,6},{8,9},{9,8},{10,11... | collective-permute-start | bytes 786440 | tf_op jit(solution)/shard_map/ppermute | solution.py:30
  29.6 54.8 %collective-permute-start.21 = (bf16[256,1024]{1,0:T(8,128)(2,1)S(1)}, bf16[256,1024]{1,0:T(8,128)(2,1)}, u32[]{:S(2)}, u32[]{:S(2)}) collective-permute-start(bf16[256,1024]{1,0:T(8,128)(2,1)S(1)} %collective-permute-done.20.refs_6_), channel_id=1, source_target_pairs={{0,1},{1,0},{2,3},{3,2},{4,5},{5,4},{6,7},{7,6},{8,9},{9,8},{10,11... | collective-permute-start | bytes 1572872 | tf_op jit(solution)/shard_map/ppermute | solution.py:30
  37.6 31.4 %copy-start.1 = (bf16[1024,256]{1,0:T(8,128)(2,1)S(1)}, bf16[1024,256]{1,0:T(8,128)(2,1)}, u32[]{:S(2)}) copy-start(bf16[1024,256]{1,0:T(8,128)(2,1)} %out_gate_w.1) | copy-start | bytes 1572868
  45.0 11.3 %collective-permute-start.4 = (bf16[2,32,128]{2,1,0:T(8,128)(2,1)S(1)}, bf16[2,32,128]{2,1,0:T(8,128)(2,1)S(1)}, u32[]{:S(2)}, u32[]{:S(2)}) collective-permute-start(bf16[2,32,128]{2,1,0:T(8,128)(2,1)S(1)} %get-tuple-element.26), channel_id=1, source_target_pairs={{0,8},{1,9},{2,10},{3,11},{4,12},{5,13},{6,14},{7,15},{8,16},{9,17... | collective-permute-start | bytes 49160 | tf_op jit(solution)/shard_map/ppermute | solution.py:30
  49.2 15.3 %collective-permute-start.12 = (bf16[2,2,144,128]{3,2,1,0:T(8,128)(2,1)}, bf16[2,2,144,128]{3,2,1,0:T(8,128)(2,1)S(1)}, u32[]{:S(2)}, u32[]{:S(2)}) collective-permute-start(bf16[2,2,144,128]{3,2,1,0:T(8,128)(2,1)} %get-tuple-element.31), channel_id=1, source_target_pairs={{0,8},{1,9},{2,10},{3,11},{4,12},{5,13},{6,14},{7,15},{8,16},{9,17... | collective-permute-start | bytes 442376 | tf_op jit(solution)/shard_map/ppermute | solution.py:30
  52.7 14.1 %collective-permute-start.13 = (bf16[2,2,144,128]{3,2,1,0:T(8,128)(2,1)}, bf16[2,2,144,128]{3,2,1,0:T(8,128)(2,1)}, u32[]{:S(2)}, u32[]{:S(2)}) collective-permute-start(bf16[2,2,144,128]{3,2,1,0:T(8,128)(2,1)} %get-tuple-element.31), channel_id=1, source_target_pairs={{0,16},{1,17},{2,18},{3,19},{4,20},{5,21},{6,22},{7,23},{8,24},{9,... | collective-permute-start | bytes 442376 | tf_op jit(solution)/shard_map/ppermute | solution.py:30
  56.9 11.4 %collective-permute-start.14 = (bf16[2,2,144,128]{3,2,1,0:T(8,128)(2,1)}, bf16[2,2,144,128]{3,2,1,0:T(8,128)(2,1)}, u32[]{:S(2)}, u32[]{:S(2)}) collective-permute-start(bf16[2,2,144,128]{3,2,1,0:T(8,128)(2,1)} %get-tuple-element.31), channel_id=1, source_target_pairs={{0,24},{1,25},{2,26},{3,27},{4,28},{5,29},{6,30},{7,31}} | collective-permute-start | bytes 442376 | tf_op jit(solution)/shard_map/ppermute | solution.py:30
  63.8 11.4 %collective-permute-start.5 = (f32[136,128]{1,0:T(8,128)S(1)}, f32[136,128]{1,0:T(8,128)S(1)}, u32[]{:S(2)}, u32[]{:S(2)}) collective-permute-start(f32[136,128]{1,0:T(8,128)S(1)} %get-tuple-element.27), channel_id=1, source_target_pairs={{0,0},{1,4},{2,2},{3,6},{4,1},{5,5},{6,3},{7,7},{8,8},{9,12},{10,1... | collective-permute-start | bytes 208904 | tf_op jit(solution)/shard_map/ppermute | solution.py:30
  64.5 11.4 %collective-permute-start.6 = (f32[136,128]{1,0:T(8,128)S(1)}, f32[136,128]{1,0:T(8,128)S(1)}, u32[]{:S(2)}, u32[]{:S(2)}) collective-permute-start(f32[136,128]{1,0:T(8,128)S(1)} %get-tuple-element.28), channel_id=1, source_target_pairs={{0,4},{1,0},{2,6},{3,2},{4,5},{5,1},{6,7},{7,3},{8,12},{9,8},{10,1... | collective-permute-start | bytes 208904 | tf_op jit(solution)/shard_map/ppermute | solution.py:30
  66.8 11.8 %collective-permute-start.7 = (f32[136,128]{1,0:T(8,128)S(1)}, f32[136,128]{1,0:T(8,128)S(1)}, u32[]{:S(2)}, u32[]{:S(2)}) collective-permute-start(f32[136,128]{1,0:T(8,128)S(1)} %get-tuple-element.29), channel_id=1, source_target_pairs={{0,2},{1,6},{2,0},{3,4},{4,3},{5,7},{6,1},{7,5},{8,10},{9,14},{10,... | collective-permute-start | bytes 208904 | tf_op jit(solution)/shard_map/ppermute | solution.py:30
  68.3 11.8 %collective-permute-start.8 = (f32[136,128]{1,0:T(8,128)S(1)}, f32[136,128]{1,0:T(8,128)S(1)}, u32[]{:S(2)}, u32[]{:S(2)}) collective-permute-start(f32[136,128]{1,0:T(8,128)S(1)} %get-tuple-element.30), channel_id=1, source_target_pairs={{0,6},{1,2},{2,4},{3,0},{4,7},{5,3},{6,5},{7,1},{8,14},{9,10},{10,... | collective-permute-start | bytes 208904 | tf_op jit(solution)/shard_map/ppermute | solution.py:30
  75.2 7.0 %collective-permute-start.15 = (bf16[128,256]{1,0:T(8,128)(2,1)S(1)}, bf16[128,256]{1,0:T(8,128)(2,1)S(1)}, u32[]{:S(2)}, u32[]{:S(2)}) collective-permute-start(bf16[128,256]{1,0:T(8,128)(2,1)S(1)} %get-tuple-element.41), channel_id=1, source_target_pairs={{0,0},{1,4},{2,2},{3,6},{4,1},{5,5},{6,3},{7,7},{8,8},{9,12},{10,1... | collective-permute-start | bytes 196616 | tf_op jit(solution)/shard_map/ppermute | solution.py:30
  75.9 6.4 %collective-permute-start.16 = (bf16[128,256]{1,0:T(8,128)(2,1)S(1)}, bf16[128,256]{1,0:T(8,128)(2,1)S(1)}, u32[]{:S(2)}, u32[]{:S(2)}) collective-permute-start(bf16[128,256]{1,0:T(8,128)(2,1)S(1)} %get-tuple-element.42), channel_id=1, source_target_pairs={{0,4},{1,0},{2,6},{3,2},{4,5},{5,1},{6,7},{7,3},{8,12},{9,8},{10,1... | collective-permute-start | bytes 196616 | tf_op jit(solution)/shard_map/ppermute | solution.py:30
  78.7 4.3 %collective-permute-start.17 = (bf16[128,256]{1,0:T(8,128)(2,1)S(1)}, bf16[128,256]{1,0:T(8,128)(2,1)S(1)}, u32[]{:S(2)}, u32[]{:S(2)}) collective-permute-start(bf16[128,256]{1,0:T(8,128)(2,1)S(1)} %get-tuple-element.43), channel_id=1, source_target_pairs={{0,2},{1,6},{2,0},{3,4},{4,3},{5,7},{6,1},{7,5},{8,10},{9,14},{10,... | collective-permute-start | bytes 196616 | tf_op jit(solution)/shard_map/ppermute | solution.py:30
  80.2 4.2 %collective-permute-start.18 = (bf16[128,256]{1,0:T(8,128)(2,1)S(1)}, bf16[128,256]{1,0:T(8,128)(2,1)S(1)}, u32[]{:S(2)}, u32[]{:S(2)}) collective-permute-start(bf16[128,256]{1,0:T(8,128)(2,1)S(1)} %get-tuple-element.44), channel_id=1, source_target_pairs={{0,6},{1,2},{2,4},{3,0},{4,7},{5,3},{6,5},{7,1},{8,14},{9,10},{10,... | collective-permute-start | bytes 196616 | tf_op jit(solution)/shard_map/ppermute | solution.py:30
  (31 other events, 63.4 us)
